TPU v7x, 32 devices: a whole 2x2x4 slice. The times are simulated.
32 devices in a mesh: sp: 8 (over z, y), tp: 4 (over x, core).
Axes of the slice: x: 2, y: 2, z: 4, core: 2. Of those that a mesh axis runs over, the one named last changes fastest.
Arguments:
- tokens: bfloat16 [4096, 2048], P(('sp', 'tp')), may hold values from -6 to 6
- queries: bfloat16 [4096, 1024], P('sp', 'tp'), may hold values from -160 to 160
- keys: bfloat16 [4096, 1024], P('sp', 'tp'), may hold values from -8 to 8
- values: bfloat16 [4096, 1024], P('sp', 'tp'), may hold values from -6 to 6
- lambdas: float32 [8], P('tp'), may hold values from 0.3 to 0.8
- head_gain: float32 [128], replicated, may hold values from 0.1 to 1.9
- out_weight: bfloat16 [1024, 2048], replicated, may hold values from -0.1875 to 0.1875
- mixer_gain: float32 [2048], replicated, may hold values from 0.1 to 1.9
- up_weight: bfloat16 [2048, 4096], P('sp', 'tp'), may hold values from -0.125 to 0.125
- down_weight: bfloat16 [4096, 2048], P('tp', 'sp'), may hold values from -0.09375 to 0.09375
Outputs:
- result: bfloat16 [4096, 2048], P(('sp', 'tp'))
All inputs are finite; a program needn't handle non-finite values.
Results may differ from a plain program's by a relative error of at most 0.02.
Values may be sent and summed in bfloat16 or wider, within the bound.
A program may use at most 128 MiB of HBM per device.

v0:
```python
import math

import jax
import jax.numpy as jnp
from jax import lax
from jax.sharding import PartitionSpec as P

DQK = 64
DV = 128


def per_device(
    tokens,
    queries,
    keys,
    values,
    lambdas,
    head_gain,
    out_weight,
    mixer_gain,
    up_weight,
    down_weight,
):
    tok_rows = queries.shape[0]
    head_count = lambdas.shape[0]
    scaling = DQK ** (-0.5)
    sp_index = lax.axis_index("sp")
    first_row = sp_index * tok_rows
    last_row = first_row + tok_rows - 1
    query_split = queries.reshape(tok_rows, head_count, 2, DQK)
    query_pos = first_row + lax.broadcasted_iota(jnp.int32, (tok_rows, 1), 0)
    floor_max = jnp.full((head_count, tok_rows), -1e30, jnp.float32)
    zero_total = jnp.zeros((head_count, tok_rows), jnp.float32)
    zero_acc = jnp.zeros((head_count, tok_rows, DV), jnp.float32)
    start_state = (floor_max, zero_total, zero_acc, floor_max, zero_total, zero_acc)
    key_piece = lax.all_gather(keys, "sp", axis=0, tiled=True)
    value_piece = lax.all_gather(values, "sp", axis=0, tiled=True)
    piece_rows = key_piece.shape[0]
    block_width = math.gcd(piece_rows, 512)

    def one_block(block_index, running):
        offset = block_index * block_width

        def update(inner):
            key_block = lax.dynamic_slice_in_dim(key_piece, offset, block_width, 0).reshape(
                block_width, head_count, 2, DQK
            )
            value_block = lax.dynamic_slice_in_dim(value_piece, offset, block_width, 0).reshape(
                block_width, head_count, DV
            )
            key_pos = offset + lax.broadcasted_iota(jnp.int32, (1, block_width), 1)
            allowed = key_pos <= query_pos
            updated = []
            for map_index in range(2):
                run_max = inner[3 * map_index]
                run_total = inner[3 * map_index + 1]
                run_acc = inner[3 * map_index + 2]
                scores = (
                    jnp.einsum(
                        "qhd,khd->hqk",
                        query_split[:, :, map_index],
                        key_block[:, :, map_index],
                        preferred_element_type=jnp.float32,
                    )
                    * scaling
                )
                scores = jnp.where(allowed[None], scores, -jnp.inf)
                new_max = jnp.maximum(run_max, jnp.max(scores, axis=2))
                shrink = jnp.exp(run_max - new_max)
                exponent = jnp.exp(scores - new_max[:, :, None])
                new_total = run_total * shrink + jnp.sum(exponent, axis=2)
                new_acc = run_acc * shrink[:, :, None] + jnp.einsum(
                    "hqk,khd->hqd",
                    exponent.astype(jnp.bfloat16),
                    value_block,
                    preferred_element_type=jnp.float32,
                )
                updated += [new_max, new_total, new_acc]
            return tuple(updated)

        return lax.cond(offset <= last_row, update, lambda inner: inner, running)

    final = lax.fori_loop(0, piece_rows // block_width, one_block, start_state)
    first_map = final[2] / final[1][:, :, None]
    second_map = final[5] / final[4][:, :, None]
    differ = first_map - lambdas[:, None, None] * second_map
    spread = lax.rsqrt(jnp.mean(differ * differ, axis=2, keepdims=True) + 1e-06)
    attended = (differ * spread * head_gain).astype(jnp.bfloat16)
    attended = jnp.transpose(attended, (1, 0, 2)).reshape(tok_rows, head_count * DV)
    all_heads = lax.all_to_all(attended, "tp", split_axis=0, concat_axis=1, tiled=True)
    projected = jnp.dot(all_heads, out_weight, preferred_element_type=jnp.float32).astype(
        jnp.bfloat16
    )
    resid = (tokens.astype(jnp.float32) + projected.astype(jnp.float32)).astype(jnp.bfloat16)
    resid_full = resid.astype(jnp.float32)
    normed = (
        resid_full
        * lax.rsqrt(jnp.mean(resid_full * resid_full, axis=1, keepdims=True) + 1e-06)
        * mixer_gain
    ).astype(jnp.bfloat16)
    up_full, down_full = (
        lax.all_gather(up_weight, "sp", axis=0, tiled=True),
        lax.all_gather(down_weight, "sp", axis=1, tiled=True),
    )
    hidden = jnp.square(
        jax.nn.relu(
            jnp.dot(
                lax.all_gather(normed, "tp", axis=0, tiled=True),
                up_full,
                preferred_element_type=jnp.float32,
            )
        )
    ).astype(jnp.bfloat16)
    mixed = lax.psum_scatter(
        jnp.dot(hidden, down_full, preferred_element_type=jnp.float32).astype(jnp.bfloat16),
        "tp",
        scatter_dimension=0,
        tiled=True,
    ).astype(jnp.float32)
    return (resid_full + mixed).astype(jnp.bfloat16)


def solution(mesh):
    placed = (
        P(("sp", "tp"), None),
        P("sp", "tp"),
        P("sp", "tp"),
        P("sp", "tp"),
        P("tp"),
        P(),
        P(),
        P(),
        P("sp", "tp"),
        P("tp", "sp"),
    )
    return jax.shard_map(
        per_device, mesh=mesh, in_specs=placed, out_specs=P(("sp", "tp"), None), check_vma=False
    )
```

profile of v0, /device:TPU:25, one launch (start us, length us, event | category | flops | bytes accessed | tf_op | source)
XLA Modules:
  0.0 388.5 jit_solution(7003081648482967234)
XLA Ops:
  6.5 1.8 copy.19
  8.4 1.8 copy.21
  10.3 1.1 copy.20
  11.4 47.5 %all-gather.6.cloned.1.call-done = bf16[4096,256]{0,1:T(8,128)(2,1)} async-done(((bf16[512,256]{0,1:T(8,128)(2,1)}), bf16[4096,256]{0,1:T(8,128)(2,1)}) %all-gather.6.cloned.1.call-update) | async-done | bytes 2097168 | tf_op jit(solution)/shard_map/all_gather | solution.py:36
  58.9 50.6 %all-gather.8.cloned.1.call-done = bf16[4096,256]{0,1:T(8,128)(2,1)} async-done(((bf16[512,256]{0,1:T(8,128)(2,1)}), bf16[4096,256]{0,1:T(8,128)(2,1)}) %all-gather.8.cloned.1.call-update) | async-done | bytes 2097168 | tf_op jit(solution)/shard_map/all_gather | solution.py:37
  109.7 39.6 %while.24 = (s32[]{:T(128)}, f32[2,512]{1,0:T(2,128)S(1)}, f32[2,512]{1,0:T(2,128)S(1)}, f32[2,512,128]{2,1,0:T(8,128)S(1)}, f32[2,512]{1,0:T(2,128)S(1)}, /*ind...) while((s32[]{:T(128)}, f32[2,512]{1,0:T(2,128)S(1)}, ...), condition=%wide.region_7.8_spmd.clone, body=%wide.region_0.7_spmd.clone.sunk | while | flops 410784768 | bytes 17707416 | solution.py:83
  109.7 5.6 %conditional.3 = ((f32[2,512]{1,0:T(2,128)S(1)}, f32[2,512]{1,0:T(2,128)S(1)}, f32[2,512,128]{2,1,0:T(8,128)S(1)}, f32[2,512]{1,0:T(2,128)S(1)}, f32[2,512]{1,0:T(2,128)S(1)}, /*index=5*/f32[2,512,128]{2,1,0:T(8,128)S(1)})) conditional(s32[]{:T(128)} %convert_element_type.94, (f32[2,512]{1,0:T(2,128)S(1)}, f32[2,512]{1,0:T(2,128)S(1)}, ...), branch_computations={%region_1.0_spmd, %region_2.6_spmd} | conditional | flops 410784768 | bytes 17705066 | solution.py:81
  109.7 1.0 constant_dynamic-slice_fusion.1
  112.9 1.0 constant_dynamic-slice_fusion
  113.8 0.7 convolution_add_fusion
  114.6 0.7 convolution_add_fusion.1
  115.3 5.6 %conditional.3 = ((f32[2,512]{1,0:T(2,128)S(1)}, f32[2,512]{1,0:T(2,128)S(1)}, f32[2,512,128]{2,1,0:T(8,128)S(1)}, f32[2,512]{1,0:T(2,128)S(1)}, f32[2,512]{1,0:T(2,128)S(1)}, /*index=5*/f32[2,512,128]{2,1,0:T(8,128)S(1)})) conditional(s32[]{:T(128)} %convert_element_type.94, (f32[2,512]{1,0:T(2,128)S(1)}, f32[2,512]{1,0:T(2,128)S(1)}, ...), branch_computations={%region_1.0_spmd, %region_2.6_spmd} | conditional | flops 410784768 | bytes 17705066 | solution.py:81
  115.4 1.0 constant_dynamic-slice_fusion.1
  118.5 1.0 constant_dynamic-slice_fusion
  119.5 0.7 convolution_add_fusion
  120.2 0.7 convolution_add_fusion.1
  121.0 5.6 %conditional.3 = ((f32[2,512]{1,0:T(2,128)S(1)}, f32[2,512]{1,0:T(2,128)S(1)}, f32[2,512,128]{2,1,0:T(8,128)S(1)}, f32[2,512]{1,0:T(2,128)S(1)}, f32[2,512]{1,0:T(2,128)S(1)}, /*index=5*/f32[2,512,128]{2,1,0:T(8,128)S(1)})) conditional(s32[]{:T(128)} %convert_element_type.94, (f32[2,512]{1,0:T(2,128)S(1)}, f32[2,512]{1,0:T(2,128)S(1)}, ...), branch_computations={%region_1.0_spmd, %region_2.6_spmd} | conditional | flops 410784768 | bytes 17705066 | solution.py:81
  121.0 1.0 constant_dynamic-slice_fusion.1
  124.1 1.0 constant_dynamic-slice_fusion
  125.1 0.7 convolution_add_fusion
  125.8 0.7 convolution_add_fusion.1
  126.6 5.6 %conditional.3 = ((f32[2,512]{1,0:T(2,128)S(1)}, f32[2,512]{1,0:T(2,128)S(1)}, f32[2,512,128]{2,1,0:T(8,128)S(1)}, f32[2,512]{1,0:T(2,128)S(1)}, f32[2,512]{1,0:T(2,128)S(1)}, /*index=5*/f32[2,512,128]{2,1,0:T(8,128)S(1)})) conditional(s32[]{:T(128)} %convert_element_type.94, (f32[2,512]{1,0:T(2,128)S(1)}, f32[2,512]{1,0:T(2,128)S(1)}, ...), branch_computations={%region_1.0_spmd, %region_2.6_spmd} | conditional | flops 410784768 | bytes 17705066 | solution.py:81
  126.7 1.0 constant_dynamic-slice_fusion.1
  129.8 1.0 constant_dynamic-slice_fusion
  130.8 0.7 convolution_add_fusion
  131.5 0.7 convolution_add_fusion.1
  132.3 5.6 %conditional.3 = ((f32[2,512]{1,0:T(2,128)S(1)}, f32[2,512]{1,0:T(2,128)S(1)}, f32[2,512,128]{2,1,0:T(8,128)S(1)}, f32[2,512]{1,0:T(2,128)S(1)}, f32[2,512]{1,0:T(2,128)S(1)}, /*index=5*/f32[2,512,128]{2,1,0:T(8,128)S(1)})) conditional(s32[]{:T(128)} %convert_element_type.94, (f32[2,512]{1,0:T(2,128)S(1)}, f32[2,512]{1,0:T(2,128)S(1)}, ...), branch_computations={%region_1.0_spmd, %region_2.6_spmd} | conditional | flops 410784768 | bytes 17705066 | solution.py:81
  132.3 1.0 constant_dynamic-slice_fusion.1
  135.4 1.0 constant_dynamic-slice_fusion
  136.4 0.7 convolution_add_fusion
  137.9 5.6 %conditional.3 = ((f32[2,512]{1,0:T(2,128)S(1)}, f32[2,512]{1,0:T(2,128)S(1)}, f32[2,512,128]{2,1,0:T(8,128)S(1)}, f32[2,512]{1,0:T(2,128)S(1)}, f32[2,512]{1,0:T(2,128)S(1)}, /*index=5*/f32[2,512,128]{2,1,0:T(8,128)S(1)})) conditional(s32[]{:T(128)} %convert_element_type.94, (f32[2,512]{1,0:T(2,128)S(1)}, f32[2,512]{1,0:T(2,128)S(1)}, ...), branch_computations={%region_1.0_spmd, %region_2.6_spmd} | conditional | flops 410784768 | bytes 17705066 | solution.py:81
  137.9 1.0 constant_dynamic-slice_fusion.1
  141.1 1.0 constant_dynamic-slice_fusion
  142.1 0.7 convolution_add_fusion
  142.8 0.7 convolution_add_fusion.1
  143.6 5.6 %conditional.3 = ((f32[2,512]{1,0:T(2,128)S(1)}, f32[2,512]{1,0:T(2,128)S(1)}, f32[2,512,128]{2,1,0:T(8,128)S(1)}, f32[2,512]{1,0:T(2,128)S(1)}, f32[2,512]{1,0:T(2,128)S(1)}, /*index=5*/f32[2,512,128]{2,1,0:T(8,128)S(1)})) conditional(s32[]{:T(128)} %convert_element_type.94, (f32[2,512]{1,0:T(2,128)S(1)}, f32[2,512]{1,0:T(2,128)S(1)}, ...), branch_computations={%region_1.0_spmd, %region_2.6_spmd} | conditional | flops 410784768 | bytes 17705066 | solution.py:81
  143.6 1.0 constant_dynamic-slice_fusion.1
  146.7 1.0 constant_dynamic-slice_fusion
  147.7 0.7 convolution_add_fusion
  150.5 8.1 %all_to_all.19 = bf16[4,128,256]{2,1,0:T(8,128)(2,1)S(1)} all-to-all(bf16[4,128,256]{2,1,0:T(8,128)(2,1)S(1)} %all_to_all.14), channel_id=1, replica_groups=mesh['sp'=8,'tp'=4] {'tp'}, dimensions={0} | all-to-all | bytes 524288 | tf_op jit(solution)/shard_map/all_to_all | solution.py:90
  158.8 3.0 multiply_reduce_fusion
  161.8 1.0 multiply_convert_fusion.1
  164.0 26.9 %all-gather.10.cloned.1.call-done = bf16[512,2048]{1,0:T(8,128)(2,1)} async-done(((bf16[128,2048]{1,0:T(8,128)(2,1)}), bf16[512,2048]{1,0:T(8,128)(2,1)}) %all-gather.10.cloned.1.call-update) | async-done | bytes 2097168 | tf_op jit(solution)/shard_map/all_gather | solution.py:108
  190.9 72.8 %all-gather.12.cloned.1.call-done = bf16[2048,1024]{1,0:T(8,128)(2,1)} async-done(((bf16[256,1024]{1,0:T(8,128)(2,1)}), bf16[2048,1024]{1,0:T(8,128)(2,1)}) %all-gather.12.cloned.1.call-update) | async-done | bytes 4194320 | tf_op jit(solution)/shard_map/all_gather | solution.py:102
  263.8 74.8 %all-gather.14.cloned.1.call-done = bf16[1024,2048]{1,0:T(8,128)(2,1)} async-done(((bf16[1024,256]{1,0:T(8,128)(2,1)}), bf16[1024,2048]{1,0:T(8,128)(2,1)}) %all-gather.14.cloned.1.call-update) | async-done | bytes 4194320 | tf_op jit(solution)/shard_map/all_gather | solution.py:103
  338.6 9.9 %convolution_convert_fusion = bf16[512,2048]{1,0:T(8,128)(2,1)} fusion(bf16[1024,2048]{1,0:T(8,128)(2,1)} %all-gather.14.cloned.1.call-done, bf16[512,2048]{1,0:T(8,128)(2,1)} %all-gather.10.cloned.1.call-done, bf16[2048,1024]{1,0:T(8,128)(2,1)} %all-gather.12.cloned.1.call-done), kind=kOutput, calls=%fused_computation.28 | convolution fusion | flops 4297588736 | bytes 12582912 | tf_op jit(solution)/shard_map/dot_general | solution.py:115
  348.6 31.2 %reduce-scatter.2.cloned.1.call-done = bf16[128,2048]{1,0:T(8,128)(2,1)} async-done(((bf16[512,2048]{1,0:T(8,128)(2,1)}), bf16[128,2048]{1,0:T(8,128)(2,1)}) %reduce-scatter.2.cloned.1.call-update) | async-done | bytes 524304 | tf_op jit(solution)/shard_map/reduce_scatter | solution.py:114
  379.7 1.9 add_convert_fusion
  (129 shorter events, 19.1 us)
Async XLA Ops:
  6.5 52.4 %all-gather.6.cloned.1.call-start = ((), (), s32[]{:S(2)}) async-start(), calls=%async_computation.2 | async-start | bytes 2359296 | tf_op jit(solution)/shard_map/all_gather | solution.py:36
  8.4 101.1 %all-gather.8.cloned.1.call-start = ((), (), s32[]{:S(2)}) async-start(), calls=%async_computation.3 | async-start | bytes 2359296 | tf_op jit(solution)/shard_map/all_gather | solution.py:37
  10.2 180.7 %all-gather.10.cloned.1.call-start = ((), (), s32[]{:S(2)}) async-start(), calls=%async_computation.4 | async-start | bytes 2621440 | tf_op jit(solution)/shard_map/all_gather | solution.py:108
  109.6 39.6 %copy-start.2 = (f32[2]{0:T(128)S(1)}, f32[2]{0:T(128)}, u32[]{:S(2)}) copy-start(f32[2]{0:T(128)} %param.18) | copy-start | bytes 28
  109.6 40.1 %copy-start.3 = (f32[128]{0:T(128)S(1)}, f32[128]{0:T(128)}, u32[]{:S(2)}) copy-start(f32[128]{0:T(128)} %param.19) | copy-start | bytes 1540
  149.2 9.5 %copy-start = (bf16[128,2048]{1,0:T(8,128)(2,1)S(1)}, bf16[128,2048]{1,0:T(8,128)(2,1)}, u32[]{:S(2)}) copy-start(bf16[128,2048]{1,0:T(8,128)(2,1)} %param.14) | copy-start | bytes 1572868
  158.8 3.0 copy-start.1
  162.8 101.0 %all-gather.12.cloned.1.call-start = ((), (), s32[]{:S(2)}) async-start(), calls=%async_computation.5 | async-start | bytes 4718592 | tf_op jit(solution)/shard_map/all_gather | solution.py:102
  163.4 175.2 %all-gather.14.cloned.1.call-start = ((), (), s32[]{:S(2)}) async-start(), calls=%async_computation.6 | async-start | bytes 4718592 | tf_op jit(solution)/shard_map/all_gather | solution.py:103
  164.0 215.8 %reduce-scatter.2.cloned.1.call-start = ((), (), s32[]{:S(2)}) async-start(), calls=%async_computation.7 | async-start | bytes 2621440 | tf_op jit(solution)/shard_map/reduce_scatter | solution.py:114
Sparse Core Ops, SparseCore 0:
  9.4 49.4 all-gather.5
  60.9 48.5 all-gather.7
  162.9 27.9 all-gather.9
  192.9 70.8 all-gather.11
  265.7 72.8 all-gather.13
  348.7 31.0 reduce-scatter.1
where the time goes:
time: 391 us; the launch traced here: 389 us
  waiting for transfers between devices  305 us (78%)
  matrix products  31.7 us (8%)
  local copies, waits for them, and re-layouts  19.1 us (5%)
  between operations  13.6 us (3%)
  other arithmetic  9.66 us (2%)
  blocking collectives  8.12 us (2%)
    all_gather x1, waiting for transfers between devices, per_device(): lax.all_gather(down_weight, 'sp', axis=1, tiled=True)  74.8 us
    all_gather x1, waiting for transfers between devices, per_device(): lax.all_gather(up_weight, 'sp', axis=0, tiled=True)  72.8 us
    all_gather x1, waiting for transfers between devices, per_device(): value_piece = lax.all_gather(values, 'sp', axis=0, tiled=True)  50.6 us
    all_gather x1, waiting for transfers between devices, per_device(): key_piece = lax.all_gather(keys, 'sp', axis=0, tiled=True)  47.5 us
    reduce_scatter x1, waiting for transfers between devices, per_device(): lax.psum_scatter(jnp.dot(hidden, down_full, preferred_element_type=jnp.fl...  31.2 us
    all_gather x1, waiting for transfers between devices, per_device(): lax.all_gather(normed, 'tp', axis=0, tiled=True)  26.9 us
    dot_general x14, matrix products, update(): jnp.einsum('hqk,khd->hqd', exponent.astype(jnp.bfloat16), value_block, pr...  9.99 us
    dot_general x1, matrix products, per_device(): jnp.dot(hidden, down_full, preferred_element_type=jnp.float32)  9.93 us
  transfers between devices with their start and end apart: 6, of which 6 were waited for; matrix products, arithmetic and copies ran while one was open for 1% of the time, Pallas kernels for 0%

commit v1 on v0

v1 whole, which is shorter than its diff:
```python
import functools

import jax
import jax.numpy as jnp
from jax import lax
from jax.experimental import pallas as pl
from jax.experimental.pallas import tpu as pltpu
from jax.sharding import PartitionSpec as P

DQK = 64
MESH = pl.DeviceIdType.MESH
f32, bf16 = jnp.float32, jnp.bfloat16


def front_kernel(
    n, tp,
    lam_ref, q_ref, k_ref, v_ref, gain_ref, up_ref, dn_ref,
    ah_ref, upf_ref, dnf_ref,
    qb, kv, qm, run_max, run_sum, acc, att,
    ex_send, ex_recv, kv_send, kv_recv, w_send, own_send, y_send, w_recv, a_send, a_recv, loc,
):
    s = lax.axis_index("sp")
    t = lax.axis_index("tp")
    z, y = s // 2, lax.rem(s, 2)
    steps = n // 2
    rows = q_ref.shape[0]
    wide = q_ref.shape[1] // 2
    peer = (s + 1 - 2 * y, t)
    above, below = (s + 2, t), (s - 2, t)
    has_up, has_down = z < steps - 1, z > 0
    piece = rows // tp

    barrier = pltpu.get_barrier_semaphore()

    def greet(device):
        pl.semaphore_signal(barrier, inc=1, device_id=device, device_id_type=MESH)

    for e in range(2):
        for i in range(tp):
            who = (2 * z + e, i)

            @pl.when(jnp.logical_or(e != y, i != t))
            def _():
                greet(who)

    pl.when(has_up)(lambda: greet(above))
    pl.when(has_down)(lambda: greet(below))
    pl.semaphore_wait(barrier, 2 * tp - 1 + has_up.astype(jnp.int32) + has_down.astype(jnp.int32))

    def remote(src, dst, send, recv, device):
        return pltpu.make_async_remote_copy(
            src_ref=src, dst_ref=dst, send_sem=send, recv_sem=recv, device_id=device, device_id_type=MESH
        )

    my_rows = pl.ds(pl.multiple_of(y * rows, rows), rows)
    peer_rows = pl.ds(pl.multiple_of((1 - y) * rows, rows), rows)
    my_cols = pl.ds(pl.multiple_of(y * wide, wide), wide)
    peer_cols = pl.ds(pl.multiple_of((1 - y) * wide, wide), wide)
    ex = []
    for i, (src, dst) in enumerate(((k_ref, kv.at[z, 0]), (v_ref, kv.at[z, 1]), (q_ref, qb))):
        ex.append(remote(src.at[:, peer_cols], dst.at[my_rows], ex_send.at[i], ex_recv.at[i], peer))
        ex[-1].start()

    def shard(ref_index, j):
        if ref_index == 0:
            depth = up_ref.shape[0]
            return upf_ref.at[pl.ds(pl.multiple_of(j * depth, depth), depth)]
        return dnf_ref.at[j]

    own = (up_ref, dn_ref)
    for c in range(2):

        @pl.when(has_down)
        def _():
            remote(own[c], shard(c, s), own_send.at[c], w_recv.at[s, c], below).start()

        remote(own[c], shard(c, s), y_send.at[s, c], w_recv.at[s, c], peer).start()
    local = []
    for i, (src, dst) in enumerate(
        (
            (k_ref.at[:, my_cols], kv.at[z, 0, my_rows]),
            (v_ref.at[:, my_cols], kv.at[z, 1, my_rows]),
            (q_ref.at[:, my_cols], qb.at[my_rows]),
            (up_ref, shard(0, s)),
            (dn_ref, shard(1, s)),
        )
    ):
        local.append(pltpu.make_async_copy(src, dst, loc.at[i]))
        local[-1].start()
    for i in range(3):
        local[i].wait()
    for i, (src, dst) in enumerate(((k_ref, kv.at[z, 0]), (v_ref, kv.at[z, 1]), (q_ref, qb))):
        remote(src.at[:, peer_cols], dst.at[peer_rows], ex_send.at[i], ex_recv.at[i], peer).wait_recv()

    def own_up():
        for c in range(2):
            remote(own[c], shard(c, s), w_send.at[s, c], w_recv.at[s, c], above).start()

    def kv_forward(j):
        return remote(kv.at[j], kv.at[j], kv_send.at[j], kv_recv.at[j], above)

    @pl.when(has_up)
    def _():
        kv_forward(z).start()
        pl.when(z == 0)(own_up)

    total = 2 * rows
    lane = lax.broadcasted_iota(jnp.int32, (total, wide), 1)
    scaled = qb[...] * jnp.asarray(DQK ** -0.5, bf16)
    for m in range(2):
        qm[m * total:(m + 1) * total, :] = jnp.where((lane < DQK) == (m == 0), scaled, jnp.zeros_like(scaled))

    chunk = min(256, total)

    def scores_of(r0, j, keys):
        return lax.dot_general(
            qm[pl.ds(r0, chunk), :], kv[j, 0, :keys, :], (((1,), (1,)), ((), ())), preferred_element_type=f32
        )

    for m in range(2):
        for b in range(total // chunk):
            r0, keys = m * total + b * chunk, (b + 1) * chunk
            sc = scores_of(r0, z, keys)
            qpos = b * chunk + lax.broadcasted_iota(jnp.int32, (chunk, keys), 0)
            kpos = lax.broadcasted_iota(jnp.int32, (chunk, keys), 1)
            sc = jnp.where(kpos <= qpos, sc, -jnp.inf)
            top = jnp.max(sc, axis=1, keepdims=True)
            p = jnp.exp(sc - top)
            run_max[pl.ds(r0, chunk), :] = jnp.broadcast_to(top, (chunk, 128))
            run_sum[pl.ds(r0, chunk), :] = jnp.broadcast_to(jnp.sum(p, axis=1, keepdims=True), (chunk, 128))
            acc[pl.ds(r0, chunk), :] = jnp.dot(p.astype(bf16), kv[z, 1, :keys, :], preferred_element_type=f32)

    def block(d, carry):
        j = z - d
        kv_forward(j).wait_recv()

        @pl.when(has_up)
        def _():
            kv_forward(j).start()
            pl.when(j == 0)(own_up)

        def part(b, inner):
            r0 = pl.multiple_of(b * chunk, chunk)
            here = pl.ds(r0, chunk)
            sc = scores_of(r0, j, total)
            old = run_max[here, :]
            top = jnp.maximum(old, jnp.max(sc, axis=1, keepdims=True))
            p = jnp.exp(sc - top[:, :1])
            shrink = jnp.exp(old - top)
            run_max[here, :] = top
            run_sum[here, :] = run_sum[here, :] * shrink + jnp.sum(p, axis=1, keepdims=True)
            acc[here, :] = acc[here, :] * shrink + jnp.dot(p.astype(bf16), kv[j, 1], preferred_element_type=f32)
            return inner

        return lax.fori_loop(0, 2 * total // chunk, part, carry)

    lax.fori_loop(1, z + 1, block, 0)

    lam = lam_ref[y]
    differ = acc[:total, :] / run_sum[:total, :] - lam * (acc[total:, :] / run_sum[total:, :])
    spread = lax.rsqrt(jnp.mean(differ * differ, axis=1, keepdims=True) + 1e-06)
    att[...] = (differ * spread * gain_ref[...]).astype(bf16)

    head = 2 * t + y
    head_cols = pl.ds(pl.multiple_of(head * wide, wide), wide)

    def to_token(e, i, head_index):
        cols = pl.ds(pl.multiple_of(head_index * wide, wide), wide)
        return remote(
            att.at[pl.ds(e * rows + i * piece, piece)], ah_ref.at[:, cols],
            a_send.at[e * tp + i], a_recv.at[head_index], (2 * z + e, i),
        )

    mine = pltpu.make_async_copy(
        att.at[pl.ds(pl.multiple_of(y * rows + t * piece, piece), piece)], ah_ref.at[:, head_cols], loc.at[5]
    )
    mine.start()
    for e in range(2):
        for i in range(tp):
            pl.when(jnp.logical_or(e != y, i != t))(lambda: to_token(e, i, head).start())

    def arrive(j, onward, exists):
        for c in range(2):
            for e in range(1):
                moved = shard(c, j)

                @pl.when(jnp.logical_or(j > s, j < s))
                def _():
                    remote(moved, moved, w_send.at[j, c], w_recv.at[j, c], peer).wait_recv()
                    remote(moved, moved, y_send.at[j, c], w_recv.at[j, c], peer).start()
                    pl.when(exists)(lambda: remote(moved, moved, w_send.at[j, c], w_recv.at[j, c], onward).start())

    def pump(d, carry):
        pl.when(z + d < steps)(lambda: arrive(s + 2 * d, below, has_down))
        pl.when(z - d >= 0)(lambda: arrive(s - 2 * d, above, has_up))
        return carry

    lax.fori_loop(1, steps, pump, 0)

    def across(i, carry):
        j = 2 * i + 1 - y
        for c in range(2):
            remote(shard(c, j), shard(c, j), y_send.at[j, c], w_recv.at[j, c], peer).wait_recv()
        return carry

    lax.fori_loop(0, steps, across, 0)
    for i in range(2 * tp):
        e, who = i % 2, i // 2
        pl.when(jnp.logical_or(e != y, who != t))(lambda: to_token(0, 0, i).wait_recv())

    mine.wait()
    local[3].wait()
    local[4].wait()
    for copy in ex:
        copy.wait_send()
    for e in range(2):
        for i in range(tp):
            pl.when(jnp.logical_or(e != y, i != t))(lambda: to_token(e, i, head).wait_send())

    @pl.when(has_up)
    def _():
        def sent(j, carry):
            kv_forward(j).wait_send()
            return carry

        lax.fori_loop(0, z + 1, sent, 0)

    def line_sent(i, carry):
        j = 2 * i + y
        for c in range(2):
            moved = shard(c, j)
            remote(moved, moved, y_send.at[j, c], w_recv.at[j, c], peer).wait_send()
            gone = jnp.logical_or(jnp.logical_and(i <= z, has_up), jnp.logical_and(i > z, has_down))
            pl.when(gone)(lambda: remote(moved, moved, w_send.at[j, c], w_recv.at[j, c], peer).wait_send())
        return carry

    lax.fori_loop(0, steps, line_sent, 0)

    @pl.when(has_down)
    def _():
        for c in range(2):
            remote(own[c], shard(c, s), own_send.at[c], w_recv.at[s, c], below).wait_send()


def front(n, tp, lambdas, queries, keys, values, head_gain, up_weight, down_weight):
    rows, wide = queries.shape[0], queries.shape[1] // 2
    depth, hid = up_weight.shape
    cols = down_weight.shape[1]
    vmem = pl.BlockSpec(memory_space=pltpu.VMEM)
    dma = pltpu.SemaphoreType.DMA
    return pl.pallas_call(
        functools.partial(front_kernel, n, tp),
        out_shape=(
            jax.ShapeDtypeStruct((rows // tp, 2 * tp * wide), bf16),
            jax.ShapeDtypeStruct((n * depth, hid), bf16),
            jax.ShapeDtypeStruct((n, hid, cols), bf16),
        ),
        in_specs=[pl.BlockSpec(memory_space=pltpu.SMEM)] + [vmem] * 6,
        out_specs=(vmem, vmem, vmem),
        scratch_shapes=[
            pltpu.VMEM((2 * rows, wide), bf16),
            pltpu.VMEM((n // 2, 2, 2 * rows, wide), bf16),
            pltpu.VMEM((4 * rows, wide), bf16),
            pltpu.VMEM((4 * rows, 128), f32),
            pltpu.VMEM((4 * rows, 128), f32),
            pltpu.VMEM((4 * rows, wide), f32),
            pltpu.VMEM((2 * rows, wide), bf16),
            dma((3,)), dma((3,)), dma((n // 2,)), dma((n // 2,)),
            dma((n, 2)), dma((2,)), dma((n, 2)), dma((n, 2)), dma((2 * tp,)), dma((2 * tp,)), dma((6,)),
        ],
        compiler_params=pltpu.CompilerParams(
            collective_id=0, has_side_effects=True, vmem_limit_bytes=60 * 1024 * 1024
        ),
    )(lambdas, queries, keys, values, head_gain.reshape(1, -1), up_weight, down_weight)


def per_device(
    n, tp, tokens, queries, keys, values, lambdas, head_gain, out_weight, mixer_gain, up_weight, down_weight
):
    all_heads, up_full, down_full = front(
        n, tp, lambdas, queries, keys, values, head_gain, up_weight, down_weight
    )
    down_full = jnp.transpose(down_full, (1, 0, 2)).reshape(down_full.shape[1], -1)
    projected = jnp.dot(all_heads, out_weight, preferred_element_type=f32).astype(bf16)
    resid = (tokens.astype(f32) + projected.astype(f32)).astype(bf16)
    resid_full = resid.astype(f32)
    normed = (
        resid_full
        * lax.rsqrt(jnp.mean(resid_full * resid_full, axis=1, keepdims=True) + 1e-06)
        * mixer_gain
    ).astype(bf16)
    hidden = jnp.square(
        jax.nn.relu(
            jnp.dot(lax.all_gather(normed, "tp", axis=0, tiled=True), up_full, preferred_element_type=f32)
        )
    ).astype(bf16)
    mixed = lax.psum_scatter(
        jnp.dot(hidden, down_full, preferred_element_type=f32).astype(bf16),
        "tp",
        scatter_dimension=0,
        tiled=True,
    ).astype(f32)
    return (resid_full + mixed).astype(bf16)


def solution(mesh):
    placed = (
        P(("sp", "tp"), None),
        P("sp", "tp"),
        P("sp", "tp"),
        P("sp", "tp"),
        P("tp"),
        P(),
        P(),
        P(),
        P("sp", "tp"),
        P("tp", "sp"),
    )
    return jax.shard_map(
        functools.partial(per_device, mesh.shape["sp"], mesh.shape["tp"]),
        mesh=mesh,
        in_specs=placed,
        out_specs=P(("sp", "tp"), None),
        check_vma=False,
    )
```

time: 391 us -> 218 us (0.56)
  waiting for transfers between devices: 305 us -> 52.4 us
  Pallas kernels: 0 us -> 128 us
  matrix products: 31.7 us -> 13.1 us
  local copies, waits for them, and re-layouts: 19.1 us -> 6.52 us
  blocking collectives: 8.12 us -> 0 us
  other arithmetic: 9.66 us -> 2.9 us
    all_gather x4 -> x0, waiting for transfers between devices: 246 us -> none  [the longest x1 74.8 us: per_device(): lax.all_gather(down_weight, 'sp', axis=1, tiled=True)]
    pallas_call x0 -> x1, Pallas kernels: none -> 128 us  [front(): pl.pallas_call(functools.partial(front_kernel, n, tp), out_shape=(jax.Sha...]
    dot_general x30 -> x2, matrix products: 31.7 us -> 13.1 us  [the longest x1 9.88 us: per_device(): jnp.dot(hidden, down_full, preferred_element_type=f32).astype(bf16)]
    dynamic_slice x14 -> x0, local copies, waits for them, and re-layouts: 13.6 us -> none  [the longest x7 6.83 us: update(): lax.dynamic_slice_in_dim(value_piece, offset, block_width, 0)]
    all_to_all x1 -> x0, blocking collectives: 8.12 us -> none  [per_device(): lax.all_to_all(attended, 'tp', split_axis=0, concat_axis=1, tiled=True)]
    transpose x1, local copies, waits for them, and re-layouts: 0.27 us -> 6.52 us  [per_device(): jnp.transpose(down_full, (1, 0, 2)).reshape(down_full.shape[1], -1)]
    all_gather x1, waiting for transfers between devices: 26.9 us -> 21.6 us  [per_device(): lax.all_gather(normed, 'tp', axis=0, tiled=True)]
    reduce_sum x15 -> x0, other arithmetic: 4.74 us -> none  [the longest x14 4.23 us: update(): new_total = run_total * shrink + jnp.sum(exponent, axis=2)]
  transfers between devices with their start and end apart: 6 -> 2, of which waited for: 6 -> 2; matrix products, arithmetic and copies ran while one was open for 1% -> 3% of each run, Pallas kernels for 0% -> 0%
where the time goes in v1:
time: 218 us; the launch traced here: 216 us
  Pallas kernels  128 us (59%)
  waiting for transfers between devices  52.4 us (24%)
  between operations  13.4 us (6%)
  matrix products  13.1 us (6%)
  local copies, waits for them, and re-layouts  6.52 us (3%)
  other arithmetic  2.9 us (1%)
    pallas_call x1, Pallas kernels, front(): pl.pallas_call(functools.partial(front_kernel, n, tp), out_shape=(jax.Sha...  128 us
    reduce_scatter x1, waiting for transfers between devices, per_device(): lax.psum_scatter(jnp.dot(hidden, down_full, preferred_element_type=f32).a...  30.8 us
    all_gather x1, waiting for transfers between devices, per_device(): lax.all_gather(normed, 'tp', axis=0, tiled=True)  21.6 us
    dot_general x1, matrix products, per_device(): jnp.dot(hidden, down_full, preferred_element_type=f32).astype(bf16)  9.88 us
    transpose x1, local copies, waits for them, and re-layouts, per_device(): jnp.transpose(down_full, (1, 0, 2)).reshape(down_full.shape[1], -1)  6.52 us
  transfers between devices with their start and end apart: 2, of which 2 were waited for; matrix products, arithmetic and copies ran while one was open for 3% of the time, Pallas kernels for 0%

profile of v1, /device:TPU:25, one launch (start us, length us, event | category | flops | bytes accessed | tf_op | source)
XLA Modules:
  0.0 216.0 jit_solution(16480394596827306012)
XLA Ops:
  6.5 0.0 copy-start
  6.5 0.0 all-gather.2.cloned.1.call-start
  6.5 127.6 %shard_map.100 = (bf16[128,1024]{1,0:T(8,128)(2,1)}, bf16[2048,1024]{1,0:T(8,128)(2,1)}, bf16[8,1024,256]{2,1,0:T(8,128)(2,1)}) custom-call(f32[2]{0:T(128)} %lam_ref.1, bf16[512,256]{1,0:T(8,128)(2,1)} %q_ref.1, bf16[512,256]{1,0:T(8,128)(2,1)} %k_ref.1, bf16[512,256]{1,0:T(8,128)(2,1)} %v_ref.1, f32[1,128]{1,0:T(1,128)} %bitcast.10, ...), custom_call_target="tpu_custom_call" | custom-call | tf_op jit(solution)/shard_map/pallas_call | solution.py:251
  134.2 3.2 %multiply_reduce_fusion = (f32[128]{0:T(128)S(1)}, f32[128,2048]{1,0:T(8,128)S(1)}) fusion(bf16[128,1024]{1,0:T(8,128)(2,1)} %get-tuple-element.8, bf16[1024,2048]{1,0:T(8,128)(2,1)} %param.16, bf16[128,2048]{1,0:T(8,128)(2,1)} %param.10), kind=kOutput, calls=%fused_computation.9 | convolution fusion | flops 538967936 | bytes 6029824 | tf_op jit(solution)/shard_map/dot_general | solution.py:284
  137.4 0.0 copy-done
  137.4 0.9 multiply_convert_fusion.1
  138.4 0.0 all-gather.2.cloned.1.call-update
  138.4 0.0 reduce-scatter.2.cloned.1.call-start
  138.5 6.5 %copy.11 = bf16[1024,8,256]{0,2,1:T(8,128)(2,1)} copy(bf16[1024,8,256]{2,0,1:T(8,128)(2,1)} %bitcast.8) | data formatting | bytes 8388608 | tf_op jit(solution)/shard_map/transpose | solution.py:283
  145.0 21.6 %all-gather.2.cloned.1.call-done = bf16[512,2048]{1,0:T(8,128)(2,1)} async-done(((bf16[128,2048]{1,0:T(8,128)(2,1)}), bf16[512,2048]{1,0:T(8,128)(2,1)}) %all-gather.2.cloned.1.call-update) | async-done | bytes 2097168 | tf_op jit(solution)/shard_map/all_gather | solution.py:294
  166.6 9.9 %convolution_convert_fusion = bf16[512,2048]{1,0:T(8,128)(2,1)} fusion(bf16[1024,2048]{0,1:T(8,128)(2,1)} %bitcast.9, bf16[512,2048]{1,0:T(8,128)(2,1)} %all-gather.2.cloned.1.call-done, bf16[2048,1024]{1,0:T(8,128)(2,1)} %get-tuple-element.9), kind=kOutput, calls=%fused_computation | convolution fusion | flops 4297588736 | bytes 12582912 | tf_op jit(solution)/shard_map/dot_general | solution.py:298
  176.5 0.0 reduce-scatter.2.cloned.1.call-update
  176.5 30.8 %reduce-scatter.2.cloned.1.call-done = bf16[128,2048]{1,0:T(8,128)(2,1)} async-done(((bf16[512,2048]{1,0:T(8,128)(2,1)}), bf16[128,2048]{1,0:T(8,128)(2,1)}) %reduce-scatter.2.cloned.1.call-update) | async-done | bytes 524304 | tf_op jit(solution)/shard_map/reduce_scatter | solution.py:297
  207.3 1.9 add_convert_fusion
  (1 shorter events, 0.0 us)
Async XLA Ops:
  6.5 130.9 %copy-start = (f32[2048]{0:T(1024)S(1)}, f32[2048]{0:T(1024)}, u32[]{:S(2)}) copy-start(f32[2048]{0:T(1024)} %param.17) | copy-start | bytes 24580
  6.5 160.0 %all-gather.2.cloned.1.call-start = ((), (), s32[]{:S(2)}) async-start(), calls=%async_computation.1 | async-start | bytes 2621440 | tf_op jit(solution)/shard_map/all_gather | solution.py:294
  138.4 68.9 %reduce-scatter.2.cloned.1.call-start = ((), (), s32[]{:S(2)}) async-start(), calls=%async_computation.2 | async-start | bytes 2621440 | tf_op jit(solution)/shard_map/reduce_scatter | solution.py:297
Sparse Core Ops, SparseCore 0:
  138.5 28.0 all-gather.1
  176.6 30.6 reduce-scatter.1

commit v2 on v1

--- a/solution.py
+++ b/solution.py
@@ -12,12 +12,14 @@
 f32, bf16 = jnp.float32, jnp.bfloat16
 
 
-def front_kernel(
+def layer_kernel(
     n, tp,
-    lam_ref, q_ref, k_ref, v_ref, gain_ref, up_ref, dn_ref,
+    lam_ref, q_ref, k_ref, v_ref, gain_ref, up_ref, dn_ref, tok_ref, mix_ref, ow_hbm,
+    out_ref,
     ah_ref, upf_ref, dnf_ref,
-    qb, kv, qm, run_max, run_sum, acc, att,
+    qb, kv, qm, run_max, run_sum, acc, att, ow, resid, normed, hsum, hid, part, core_in, cross, cross_in,
     ex_send, ex_recv, kv_send, kv_recv, w_send, own_send, y_send, w_recv, a_send, a_recv, loc,
+    ag_send, ag_recv, c_send, c_recv, x_send, x_recv,
 ):
     s = lax.axis_index("sp")
     t = lax.axis_index("tp")
@@ -83,6 +85,7 @@
             (q_ref.at[:, my_cols], qb.at[my_rows]),
             (up_ref, shard(0, s)),
             (dn_ref, shard(1, s)),
+            (ow_hbm, ow),
         )
     ):
         local.append(pltpu.make_async_copy(src, dst, loc.at[i]))
@@ -92,9 +95,18 @@
     for i, (src, dst) in enumerate(((k_ref, kv.at[z, 0]), (v_ref, kv.at[z, 1]), (q_ref, qb))):
         remote(src.at[:, peer_cols], dst.at[peer_rows], ex_send.at[i], ex_recv.at[i], peer).wait_recv()
 
-    def own_up():
+    def own_up(c):
+        remote(own[c], shard(c, s), w_send.at[s, c], w_recv.at[s, c], above).start()
+
+    def arrive(c, j, onward, exists):
+        moved = shard(c, j)
+        remote(moved, moved, w_send.at[j, c], w_recv.at[j, c], peer).wait_recv()
+        pl.when(exists)(lambda: remote(moved, moved, w_send.at[j, c], w_recv.at[j, c], onward).start())
+        remote(moved, moved, y_send.at[j, c], w_recv.at[j, c], peer).start()
+
+    def from_above(d):
         for c in range(2):
-            remote(own[c], shard(c, s), w_send.at[s, c], w_recv.at[s, c], above).start()
+            pl.when(z + d < steps)(lambda: arrive(c, s + 2 * d, below, has_down))
 
     def kv_forward(j):
         return remote(kv.at[j], kv.at[j], kv_send.at[j], kv_recv.at[j], above)
@@ -102,7 +114,7 @@
     @pl.when(has_up)
     def _():
         kv_forward(z).start()
-        pl.when(z == 0)(own_up)
+        pl.when(z == 0)(lambda: (own_up(0), own_up(1)) and None)
 
     total = 2 * rows
     lane = lax.broadcasted_iota(jnp.int32, (total, wide), 1)
@@ -137,9 +149,9 @@
         @pl.when(has_up)
         def _():
             kv_forward(j).start()
-            pl.when(j == 0)(own_up)
-
-        def part(b, inner):
+            pl.when(j == 0)(lambda: own_up(0))
+
+        def tile(b, inner):
             r0 = pl.multiple_of(b * chunk, chunk)
             here = pl.ds(r0, chunk)
             sc = scores_of(r0, j, total)
@@ -152,7 +164,9 @@
             acc[here, :] = acc[here, :] * shrink + jnp.dot(p.astype(bf16), kv[j, 1], preferred_element_type=f32)
             return inner
 
-        return lax.fori_loop(0, 2 * total // chunk, part, carry)
+        lax.fori_loop(0, 2 * total // chunk, tile, 0)
+        pl.when(d == 1)(lambda: from_above(1))
+        return carry
 
     lax.fori_loop(1, z + 1, block, 0)
 
@@ -172,45 +186,133 @@
         )
 
     mine = pltpu.make_async_copy(
-        att.at[pl.ds(pl.multiple_of(y * rows + t * piece, piece), piece)], ah_ref.at[:, head_cols], loc.at[5]
+        att.at[pl.ds(pl.multiple_of(y * rows + t * piece, piece), piece)], ah_ref.at[:, head_cols], loc.at[6]
     )
     mine.start()
     for e in range(2):
         for i in range(tp):
             pl.when(jnp.logical_or(e != y, i != t))(lambda: to_token(e, i, head).start())
 
-    def arrive(j, onward, exists):
-        for c in range(2):
-            for e in range(1):
-                moved = shard(c, j)
-
-                @pl.when(jnp.logical_or(j > s, j < s))
-                def _():
-                    remote(moved, moved, w_send.at[j, c], w_recv.at[j, c], peer).wait_recv()
-                    remote(moved, moved, y_send.at[j, c], w_recv.at[j, c], peer).start()
-                    pl.when(exists)(lambda: remote(moved, moved, w_send.at[j, c], w_recv.at[j, c], onward).start())
-
-    def pump(d, carry):
-        pl.when(z + d < steps)(lambda: arrive(s + 2 * d, below, has_down))
-        pl.when(z - d >= 0)(lambda: arrive(s - 2 * d, above, has_up))
-        return carry
-
-    lax.fori_loop(1, steps, pump, 0)
-
-    def across(i, carry):
-        j = 2 * i + 1 - y
-        for c in range(2):
-            remote(shard(c, j), shard(c, j), y_send.at[j, c], w_recv.at[j, c], peer).wait_recv()
-        return carry
-
-    lax.fori_loop(0, steps, across, 0)
+    def from_below(c, d):
+        @pl.when(z - d >= 0)
+        def _():
+            arrive(c, s - 2 * d, above, has_up)
+            if c == 0:
+                pl.when(jnp.logical_and(d == z, has_up))(lambda: own_up(1))
+
+    pl.when(z == 0)(lambda: from_above(1))
+    local[5].wait()
+    mine.wait()
     for i in range(2 * tp):
         e, who = i % 2, i // 2
         pl.when(jnp.logical_or(e != y, who != t))(lambda: to_token(0, 0, i).wait_recv())
 
-    mine.wait()
+    projected = jnp.dot(ah_ref[...], ow[...], preferred_element_type=f32).astype(bf16)
+    summed = (tok_ref[...].astype(f32) + projected.astype(f32)).astype(bf16)
+    resid[...] = summed
+    summed = summed.astype(f32)
+    scale = lax.rsqrt(jnp.mean(summed * summed, axis=1, keepdims=True) + 1e-06)
+
+    tc = t + 1 - 2 * lax.rem(t, 2)
+    tx = lax.rem(t + 2, tp)
+    td = lax.rem(tc + 2, tp)
+
+    def band(i):
+        return pl.ds(pl.multiple_of(i * piece, piece), piece)
+
+    normed[band(t), :] = (summed * scale * mix_ref[...]).astype(bf16)
+
+    def gathered(k, block_index, device):
+        block_ref = normed.at[band(block_index)]
+        return remote(block_ref, block_ref, ag_send.at[k], ag_recv.at[block_index], (s, device))
+
+    gathered(0, t, tx).start()
+    gathered(1, t, tc).start()
+
+    def pump(d, carry):
+        from_below(0, d)
+        pl.when(d > 1)(lambda: from_above(d))
+        return carry
+
+    lax.fori_loop(1, min(3, steps), pump, 0)
+    gathered(0, tx, tx).wait_recv()
+    gathered(2, tx, tc).start()
+    lax.fori_loop(min(3, steps), steps, pump, 0)
+    gathered(1, tc, tc).wait_recv()
+    gathered(2, td, tc).wait_recv()
     local[3].wait()
     local[4].wait()
+
+    def order(k):
+        return jnp.where(k < steps - z, z + k, steps - 1 - k)
+
+    def across(c, i):
+        j = 2 * i + 1 - y
+        remote(shard(c, j), shard(c, j), y_send.at[j, c], w_recv.at[j, c], peer).wait_recv()
+
+    pair_depth = 2 * up_ref.shape[0]
+    hsum[...] = jnp.zeros_like(hsum)
+
+    def up_pair(k, carry):
+        i = order(k)
+        across(0, i)
+        span = pl.ds(pl.multiple_of(i * pair_depth, pair_depth), pair_depth)
+        hsum[...] += jnp.dot(normed[:, span], upf_ref[span, :], preferred_element_type=f32)
+        return carry
+
+    lax.fori_loop(0, steps, up_pair, 0)
+    hid[...] = jnp.square(jnp.maximum(hsum[...], 0.0)).astype(bf16)
+
+    def to_core(j, m):
+        return remote(
+            part.at[j, band(tc if m == 0 else td)], core_in.at[j, m], c_send.at[j, m], c_recv.at[j, m], (s, tc)
+        )
+
+    def to_cross(j):
+        return remote(cross.at[j], cross_in.at[j], x_send.at[j], x_recv.at[j], (s, tx))
+
+    def add_cores(i):
+        for e in range(2):
+            j = 2 * i + e
+            to_core(j, 1).wait_recv()
+            cross[j] = (part[j, band(tx), :].astype(f32) + core_in[j, 1].astype(f32)).astype(bf16)
+            to_cross(j).start()
+
+    def down_pair(k, carry):
+        i = order(k)
+        later = order(k + 1)
+
+        @pl.when(jnp.logical_and(k + 1 < steps, later < z))
+        def _():
+            arrive(1, 2 * later + y, above, has_up)
+
+        across(1, i)
+        for e in range(2):
+            j = 2 * i + e
+            part[j] = jnp.dot(hid[...], dnf_ref[j], preferred_element_type=f32).astype(bf16)
+            to_core(j, 1).start()
+            to_core(j, 0).start()
+        pl.when(k > 0)(lambda: add_cores(order(k - 1)))
+        return carry
+
+    lax.fori_loop(0, steps, down_pair, 0)
+    add_cores(order(steps - 1))
+
+    cols = dn_ref.shape[1]
+    for j in range(n):
+        to_core(j, 0).wait_recv()
+        to_cross(j).wait_recv()
+        here = slice(j * cols, (j + 1) * cols)
+        both = part[j, band(t), :].astype(f32) + core_in[j, 0].astype(f32) + cross_in[j].astype(f32)
+        out_ref[:, here] = (resid[:, here].astype(f32) + both).astype(bf16)
+
+    gathered(0, t, tx).wait_send()
+    gathered(1, t, tc).wait_send()
+    gathered(2, tx, tc).wait_send()
+    for j in range(n):
+        to_core(j, 0).wait_send()
+        to_core(j, 1).wait_send()
+        to_cross(j).wait_send()
     for copy in ex:
         copy.wait_send()
     for e in range(2):
@@ -242,22 +344,24 @@
             remote(own[c], shard(c, s), own_send.at[c], w_recv.at[s, c], below).wait_send()
 
 
-def front(n, tp, lambdas, queries, keys, values, head_gain, up_weight, down_weight):
+def per_device(
+    n, tp, tokens, queries, keys, values, lambdas, head_gain, out_weight, mixer_gain, up_weight, down_weight
+):
     rows, wide = queries.shape[0], queries.shape[1] // 2
-    depth, hid = up_weight.shape
+    depth, units = up_weight.shape
     cols = down_weight.shape[1]
+    piece, width = tokens.shape
     vmem = pl.BlockSpec(memory_space=pltpu.VMEM)
     dma = pltpu.SemaphoreType.DMA
     return pl.pallas_call(
-        functools.partial(front_kernel, n, tp),
-        out_shape=(
-            jax.ShapeDtypeStruct((rows // tp, 2 * tp * wide), bf16),
-            jax.ShapeDtypeStruct((n * depth, hid), bf16),
-            jax.ShapeDtypeStruct((n, hid, cols), bf16),
-        ),
-        in_specs=[pl.BlockSpec(memory_space=pltpu.SMEM)] + [vmem] * 6,
-        out_specs=(vmem, vmem, vmem),
+        functools.partial(layer_kernel, n, tp),
+        out_shape=jax.ShapeDtypeStruct(tokens.shape, bf16),
+        in_specs=[pl.BlockSpec(memory_space=pltpu.SMEM)] + [vmem] * 8 + [pl.BlockSpec(memory_space=pl.ANY)],
+        out_specs=vmem,
         scratch_shapes=[
+            pltpu.VMEM((piece, 2 * tp * wide), bf16),
+            pltpu.VMEM((n * depth, units), bf16),
+            pltpu.VMEM((n, units, cols), bf16),
             pltpu.VMEM((2 * rows, wide), bf16),
             pltpu.VMEM((n // 2, 2, 2 * rows, wide), bf16),
             pltpu.VMEM((4 * rows, wide), bf16),
@@ -265,42 +369,26 @@
             pltpu.VMEM((4 * rows, 128), f32),
             pltpu.VMEM((4 * rows, wide), f32),
             pltpu.VMEM((2 * rows, wide), bf16),
+            pltpu.VMEM(out_weight.shape, bf16),
+            pltpu.VMEM((piece, width), bf16),
+            pltpu.VMEM((rows, width), bf16),
+            pltpu.VMEM((rows, units), f32),
+            pltpu.VMEM((rows, units), bf16),
+            pltpu.VMEM((n, rows, cols), bf16),
+            pltpu.VMEM((n, 2, piece, cols), bf16),
+            pltpu.VMEM((n, piece, cols), bf16),
+            pltpu.VMEM((n, piece, cols), bf16),
             dma((3,)), dma((3,)), dma((n // 2,)), dma((n // 2,)),
-            dma((n, 2)), dma((2,)), dma((n, 2)), dma((n, 2)), dma((2 * tp,)), dma((2 * tp,)), dma((6,)),
+            dma((n, 2)), dma((2,)), dma((n, 2)), dma((n, 2)), dma((2 * tp,)), dma((2 * tp,)), dma((7,)),
+            dma((3,)), dma((tp,)), dma((n, 2)), dma((n, 2)), dma((n,)), dma((n,)),
         ],
         compiler_params=pltpu.CompilerParams(
             collective_id=0, has_side_effects=True, vmem_limit_bytes=60 * 1024 * 1024
         ),
-    )(lambdas, queries, keys, values, head_gain.reshape(1, -1), up_weight, down_weight)
-
-
-def per_device(
-    n, tp, tokens, queries, keys, values, lambdas, head_gain, out_weight, mixer_gain, up_weight, down_weight
-):
-    all_heads, up_full, down_full = front(
-        n, tp, lambdas, queries, keys, values, head_gain, up_weight, down_weight
+    )(
+        lambdas, queries, keys, values, head_gain.reshape(1, -1), up_weight, down_weight,
+        tokens, mixer_gain.reshape(1, -1), out_weight,
     )
-    down_full = jnp.transpose(down_full, (1, 0, 2)).reshape(down_full.shape[1], -1)
-    projected = jnp.dot(all_heads, out_weight, preferred_element_type=f32).astype(bf16)
-    resid = (tokens.astype(f32) + projected.astype(f32)).astype(bf16)
-    resid_full = resid.astype(f32)
-    normed = (
-        resid_full
-        * lax.rsqrt(jnp.mean(resid_full * resid_full, axis=1, keepdims=True) + 1e-06)
-        * mixer_gain
-    ).astype(bf16)
-    hidden = jnp.square(
-        jax.nn.relu(
-            jnp.dot(lax.all_gather(normed, "tp", axis=0, tiled=True), up_full, preferred_element_type=f32)
-        )
-    ).astype(bf16)
-    mixed = lax.psum_scatter(
-        jnp.dot(hidden, down_full, preferred_element_type=f32).astype(bf16),
-        "tp",
-        scatter_dimension=0,
-        tiled=True,
-    ).astype(f32)
-    return (resid_full + mixed).astype(bf16)
 
 
 def solution(mesh):

time: 218 us -> 150 us (0.69)
  waiting for transfers between devices: 52.4 us -> 0 us
  Pallas kernels: 128 us -> 146 us
  between operations: 13.4 us -> 0.01 us
  matrix products: 13.1 us -> 0 us
  local copies, waits for them, and re-layouts: 6.52 us -> 1.88 us
  other arithmetic: 2.9 us -> 0 us
    reduce_scatter x1 -> x0, waiting for transfers between devices: 30.8 us -> none  [per_device(): lax.psum_scatter(jnp.dot(hidden, down_full, preferred_element_type=f32).a...]
    all_gather x1 -> x0, waiting for transfers between devices: 21.6 us -> none  [per_device(): lax.all_gather(normed, 'tp', axis=0, tiled=True)]
    pallas_call x1, Pallas kernels: 128 us -> 146 us  [per_device(): pl.pallas_call(functools.partial(layer_kernel, n, tp), out_shape=jax.Shap...]
    dot_general x2 -> x0, matrix products: 13.1 us -> none  [the longest x1 9.88 us: per_device(): jnp.dot(hidden, down_full, preferred_element_type=f32).astype(bf16)]
    transpose x1 -> x0, local copies, waits for them, and re-layouts: 6.52 us -> none  [per_device(): jnp.transpose(down_full, (1, 0, 2)).reshape(down_full.shape[1], -1)]
    convert_element_type x2 -> x0, other arithmetic: 2.89 us -> none  [the longest x1 1.94 us: per_device(): return (resid_full + mixed).astype(bf16)]
  transfers between devices with their start and end apart: 2 -> 0, of which waited for: 2 -> 0; matrix products, arithmetic and copies ran while one was open for 3% -> 0% of each run, Pallas kernels for 0% -> 0%
where the time goes in v2:
time: 150 us; the launch traced here: 148 us
  Pallas kernels  146 us (97%)
  local copies, waits for them, and re-layouts  1.88 us (1%)
    pallas_call x1, Pallas kernels, per_device(): pl.pallas_call(functools.partial(layer_kernel, n, tp), out_shape=jax.Shap...  146 us

profile of v2, /device:TPU:25, one launch (start us, length us, event | category | flops | bytes accessed | tf_op | source)
XLA Modules:
  0.0 147.7 jit_solution(14785971551585803498)
XLA Ops:
  0.0 145.8 %shard_map.100 = bf16[128,2048]{1,0:T(8,128)(2,1)} custom-call(f32[2]{0:T(128)} %lam_ref.1, bf16[512,256]{1,0:T(8,128)(2,1)} %q_ref.1, bf16[512,256]{1,0:T(8,128)(2,1)} %k_ref.1, bf16[512,256]{1,0:T(8,128)(2,1)} %v_ref.1, f32[1,128]{1,0:T(1,128)} %bitcast.3, bf16[256,1024]{1,0:T(8,128)(2,1)} %up_ref.1, bf16[1024,256]{1,0:T(8,128)(2,1)} %dn_ref.1, ...), custom_call_target="tpu_custom_call" | custom-call | tf_op jit(solution)/shard_map/pallas_call | solution.py:356
  145.8 1.9 %copy.12 = bf16[128,2048]{1,0:T(8,128)(2,1)} copy(bf16[128,2048]{1,0:T(8,128)(2,1)} %shard_map.100) | data formatting | bytes 1048576

commit v3 on v2

--- a/solution.py
+++ b/solution.py
@@ -63,14 +63,22 @@
         ex.append(remote(src.at[:, peer_cols], dst.at[my_rows], ex_send.at[i], ex_recv.at[i], peer))
         ex[-1].start()
 
-    def shard(ref_index, j):
-        if ref_index == 0:
+    half = dn_ref.shape[0] // 2
+    halves = (slice(0, half), slice(half, 2 * half))
+
+    def shard(c, j):
+        if c == 0:
             depth = up_ref.shape[0]
             return upf_ref.at[pl.ds(pl.multiple_of(j * depth, depth), depth)]
-        return dnf_ref.at[j]
-
-    own = (up_ref, dn_ref)
-    for c in range(2):
+        return dnf_ref.at[j, halves[c - 1]]
+
+    own = (up_ref, dn_ref.at[halves[0]], dn_ref.at[halves[1]])
+
+    def own_up(c):
+        remote(own[c], shard(c, s), w_send.at[s, c], w_recv.at[s, c], above).start()
+
+    pl.when(has_up)(lambda: own_up(0))
+    for c in range(3):
 
         @pl.when(has_down)
         def _():
@@ -84,7 +92,7 @@
             (v_ref.at[:, my_cols], kv.at[z, 1, my_rows]),
             (q_ref.at[:, my_cols], qb.at[my_rows]),
             (up_ref, shard(0, s)),
-            (dn_ref, shard(1, s)),
+            (dn_ref, dnf_ref.at[s]),
             (ow_hbm, ow),
         )
     ):
@@ -95,17 +103,25 @@
     for i, (src, dst) in enumerate(((k_ref, kv.at[z, 0]), (v_ref, kv.at[z, 1]), (q_ref, qb))):
         remote(src.at[:, peer_cols], dst.at[peer_rows], ex_send.at[i], ex_recv.at[i], peer).wait_recv()
 
-    def own_up(c):
-        remote(own[c], shard(c, s), w_send.at[s, c], w_recv.at[s, c], above).start()
-
-    def arrive(c, j, onward, exists):
+    def onward(c, j, device):
+        moved = shard(c, j)
+        remote(moved, moved, w_send.at[j, c], w_recv.at[j, c], device).start()
+
+    def landed(c, j):
         moved = shard(c, j)
         remote(moved, moved, w_send.at[j, c], w_recv.at[j, c], peer).wait_recv()
-        pl.when(exists)(lambda: remote(moved, moved, w_send.at[j, c], w_recv.at[j, c], onward).start())
         remote(moved, moved, y_send.at[j, c], w_recv.at[j, c], peer).start()
 
+    def arrive(c, j, device, exists):
+        landed(c, j)
+        pl.when(exists)(lambda: onward(c, j, device))
+
+    def down_up():
+        own_up(1)
+        own_up(2)
+
     def from_above(d):
-        for c in range(2):
+        for c in range(3):
             pl.when(z + d < steps)(lambda: arrive(c, s + 2 * d, below, has_down))
 
     def kv_forward(j):
@@ -114,7 +130,7 @@
     @pl.when(has_up)
     def _():
         kv_forward(z).start()
-        pl.when(z == 0)(lambda: (own_up(0), own_up(1)) and None)
+        pl.when(z == 0)(down_up)
 
     total = 2 * rows
     lane = lax.broadcasted_iota(jnp.int32, (total, wide), 1)
@@ -144,12 +160,17 @@
 
     def block(d, carry):
         j = z - d
+        pl.when(d == 1)(lambda: landed(0, s - 2))
         kv_forward(j).wait_recv()
 
         @pl.when(has_up)
         def _():
             kv_forward(j).start()
-            pl.when(j == 0)(lambda: own_up(0))
+
+            @pl.when(j == 0)
+            def _():
+                onward(0, s - 2, above)
+                pl.when(z == 1)(down_up)
 
         def tile(b, inner):
             r0 = pl.multiple_of(b * chunk, chunk)
@@ -193,12 +214,11 @@
         for i in range(tp):
             pl.when(jnp.logical_or(e != y, i != t))(lambda: to_token(e, i, head).start())
 
-    def from_below(c, d):
+    def up_below(d):
         @pl.when(z - d >= 0)
         def _():
-            arrive(c, s - 2 * d, above, has_up)
-            if c == 0:
-                pl.when(jnp.logical_and(d == z, has_up))(lambda: own_up(1))
+            arrive(0, s - 2 * d, above, has_up)
+            pl.when(jnp.logical_and(d == z, has_up))(down_up)
 
     pl.when(z == 0)(lambda: from_above(1))
     local[5].wait()
@@ -230,11 +250,11 @@
     gathered(1, t, tc).start()
 
     def pump(d, carry):
-        from_below(0, d)
-        pl.when(d > 1)(lambda: from_above(d))
+        up_below(d)
+        from_above(d)
         return carry
 
-    lax.fori_loop(1, min(3, steps), pump, 0)
+    lax.fori_loop(2, min(3, steps), pump, 0)
     gathered(0, tx, tx).wait_recv()
     gathered(2, tx, tc).start()
     lax.fori_loop(min(3, steps), steps, pump, 0)
@@ -285,14 +305,16 @@
         @pl.when(jnp.logical_and(k + 1 < steps, later < z))
         def _():
             arrive(1, 2 * later + y, above, has_up)
-
+            arrive(2, 2 * later + y, above, has_up)
+
+        pl.when(k > 0)(lambda: add_cores(order(k - 1)))
         across(1, i)
+        across(2, i)
         for e in range(2):
             j = 2 * i + e
             part[j] = jnp.dot(hid[...], dnf_ref[j], preferred_element_type=f32).astype(bf16)
             to_core(j, 1).start()
             to_core(j, 0).start()
-        pl.when(k > 0)(lambda: add_cores(order(k - 1)))
         return carry
 
     lax.fori_loop(0, steps, down_pair, 0)
@@ -329,7 +351,7 @@
 
     def line_sent(i, carry):
         j = 2 * i + y
-        for c in range(2):
+        for c in range(3):
             moved = shard(c, j)
             remote(moved, moved, y_send.at[j, c], w_recv.at[j, c], peer).wait_send()
             gone = jnp.logical_or(jnp.logical_and(i <= z, has_up), jnp.logical_and(i > z, has_down))
@@ -340,7 +362,7 @@
 
     @pl.when(has_down)
     def _():
-        for c in range(2):
+        for c in range(3):
             remote(own[c], shard(c, s), own_send.at[c], w_recv.at[s, c], below).wait_send()
 
 
@@ -379,7 +401,7 @@
             pltpu.VMEM((n, piece, cols), bf16),
             pltpu.VMEM((n, piece, cols), bf16),
             dma((3,)), dma((3,)), dma((n // 2,)), dma((n // 2,)),
-            dma((n, 2)), dma((2,)), dma((n, 2)), dma((n, 2)), dma((2 * tp,)), dma((2 * tp,)), dma((7,)),
+            dma((n, 3)), dma((3,)), dma((n, 3)), dma((n, 3)), dma((2 * tp,)), dma((2 * tp,)), dma((7,)),
             dma((3,)), dma((tp,)), dma((n, 2)), dma((n, 2)), dma((n,)), dma((n,)),
         ],
         compiler_params=pltpu.CompilerParams(

time: 150 us -> 146 us (0.973); the launches traced: 148 us -> 145 us
  Pallas kernels: 146 us -> 144 us
    pallas_call x1, Pallas kernels: 146 us -> 144 us  [per_device(): pl.pallas_call(functools.partial(layer_kernel, n, tp), out_shape=jax.Shap...]
where the time goes in v3:
time: 146 us; the launch traced here: 145 us
  Pallas kernels  144 us (99%)
  local copies, waits for them, and re-layouts  1.88 us (1%)
    pallas_call x1, Pallas kernels, per_device(): pl.pallas_call(functools.partial(layer_kernel, n, tp), out_shape=jax.Shap...  144 us

profile of v3, /device:TPU:25, one launch (start us, length us, event | category | flops | bytes accessed | tf_op | source)
XLA Modules:
  0.0 145.4 jit_solution(13504398641290050604)
XLA Ops:
  0.0 143.5 %shard_map.100 = bf16[128,2048]{1,0:T(8,128)(2,1)} custom-call(f32[2]{0:T(128)} %lam_ref.1, bf16[512,256]{1,0:T(8,128)(2,1)} %q_ref.1, bf16[512,256]{1,0:T(8,128)(2,1)} %k_ref.1, bf16[512,256]{1,0:T(8,128)(2,1)} %v_ref.1, f32[1,128]{1,0:T(1,128)} %bitcast.3, bf16[256,1024]{1,0:T(8,128)(2,1)} %up_ref.1, bf16[1024,256]{1,0:T(8,128)(2,1)} %dn_ref.1, ...), custom_call_target="tpu_custom_call" | custom-call | tf_op jit(solution)/shard_map/pallas_call | solution.py:378
  143.5 1.9 %copy.12 = bf16[128,2048]{1,0:T(8,128)(2,1)} copy(bf16[128,2048]{1,0:T(8,128)(2,1)} %shard_map.100) | data formatting | bytes 1048576

commit v4 on v3

--- a/solution.py
+++ b/solution.py
@@ -107,14 +107,24 @@
         moved = shard(c, j)
         remote(moved, moved, w_send.at[j, c], w_recv.at[j, c], device).start()
 
-    def landed(c, j):
+    def await_chunk(c, j):
         moved = shard(c, j)
         remote(moved, moved, w_send.at[j, c], w_recv.at[j, c], peer).wait_recv()
+
+    def over(c, j):
+        moved = shard(c, j)
         remote(moved, moved, y_send.at[j, c], w_recv.at[j, c], peer).start()
 
     def arrive(c, j, device, exists):
-        landed(c, j)
+        await_chunk(c, j)
+        over(c, j)
         pl.when(exists)(lambda: onward(c, j, device))
+
+    def next_above(c):
+        @pl.when(z + 1 < steps)
+        def _():
+            await_chunk(c, s + 2)
+            pl.when(has_down)(lambda: onward(c, s + 2, below))
 
     def down_up():
         own_up(1)
@@ -160,7 +170,12 @@
 
     def block(d, carry):
         j = z - d
-        pl.when(d == 1)(lambda: landed(0, s - 2))
+        @pl.when(d == 1)
+        def _():
+            await_chunk(0, s - 2)
+            over(0, s - 2)
+            next_above(0)
+
         kv_forward(j).wait_recv()
 
         @pl.when(has_up)
@@ -171,6 +186,11 @@
             def _():
                 onward(0, s - 2, above)
                 pl.when(z == 1)(down_up)
+
+        @pl.when(d == 1)
+        def _():
+            next_above(1)
+            next_above(2)
 
         def tile(b, inner):
             r0 = pl.multiple_of(b * chunk, chunk)
@@ -186,7 +206,6 @@
             return inner
 
         lax.fori_loop(0, 2 * total // chunk, tile, 0)
-        pl.when(d == 1)(lambda: from_above(1))
         return carry
 
     lax.fori_loop(1, z + 1, block, 0)
@@ -220,7 +239,17 @@
             arrive(0, s - 2 * d, above, has_up)
             pl.when(jnp.logical_and(d == z, has_up))(down_up)
 
-    pl.when(z == 0)(lambda: from_above(1))
+    @pl.when(z == 0)
+    def _():
+        for c in range(3):
+            next_above(c)
+
+    @pl.when(z + 1 < steps)
+    def _():
+        for c in range(3):
+            over(c, s + 2)
+
+    up_below(2)
     local[5].wait()
     mine.wait()
     for i in range(2 * tp):
@@ -250,7 +279,7 @@
     gathered(1, t, tc).start()
 
     def pump(d, carry):
-        up_below(d)
+        pl.when(d > 2)(lambda: up_below(d))
         from_above(d)
         return carry
 
@@ -270,6 +299,13 @@
         j = 2 * i + 1 - y
         remote(shard(c, j), shard(c, j), y_send.at[j, c], w_recv.at[j, c], peer).wait_recv()
 
+    def down_below(i):
+        @pl.when(jnp.logical_and(i >= 0, i < z))
+        def _():
+            arrive(1, 2 * i + y, above, has_up)
+            arrive(2, 2 * i + y, above, has_up)
+
+    down_below(z - 1)
     pair_depth = 2 * up_ref.shape[0]
     hsum[...] = jnp.zeros_like(hsum)
 
@@ -302,11 +338,7 @@
         i = order(k)
         later = order(k + 1)
 
-        @pl.when(jnp.logical_and(k + 1 < steps, later < z))
-        def _():
-            arrive(1, 2 * later + y, above, has_up)
-            arrive(2, 2 * later + y, above, has_up)
-
+        pl.when(jnp.logical_and(k + 1 < steps, later < z - 1))(lambda: down_below(later))
         pl.when(k > 0)(lambda: add_cores(order(k - 1)))
         across(1, i)
         across(2, i)

time: 146 us -> 139 us (0.952)
  Pallas kernels: 144 us -> 136 us
    pallas_call x1, Pallas kernels: 144 us -> 136 us  [per_device(): pl.pallas_call(functools.partial(layer_kernel, n, tp), out_shape=jax.Shap...]
where the time goes in v4:
time: 139 us; the launch traced here: 138 us
  Pallas kernels  136 us (98%)
  local copies, waits for them, and re-layouts  1.88 us (1%)
    pallas_call x1, Pallas kernels, per_device(): pl.pallas_call(functools.partial(layer_kernel, n, tp), out_shape=jax.Shap...  136 us

profile of v4, /device:TPU:25, one launch (start us, length us, event | category | flops | bytes accessed | tf_op | source)
XLA Modules:
  0.0 138.4 jit_solution(3184814893725655138)
XLA Ops:
  0.0 136.5 %shard_map.100 = bf16[128,2048]{1,0:T(8,128)(2,1)} custom-call(f32[2]{0:T(128)} %lam_ref.1, bf16[512,256]{1,0:T(8,128)(2,1)} %q_ref.1, bf16[512,256]{1,0:T(8,128)(2,1)} %k_ref.1, bf16[512,256]{1,0:T(8,128)(2,1)} %v_ref.1, f32[1,128]{1,0:T(1,128)} %bitcast.3, bf16[256,1024]{1,0:T(8,128)(2,1)} %up_ref.1, bf16[1024,256]{1,0:T(8,128)(2,1)} %dn_ref.1, ...), custom_call_target="tpu_custom_call" | custom-call | tf_op jit(solution)/shard_map/pallas_call | solution.py:410
  136.5 1.9 %copy.12 = bf16[128,2048]{1,0:T(8,128)(2,1)} copy(bf16[128,2048]{1,0:T(8,128)(2,1)} %shard_map.100) | data formatting | bytes 1048576

commit v5 on v4

--- a/solution.py
+++ b/solution.py
@@ -140,7 +140,7 @@
     @pl.when(has_up)
     def _():
         kv_forward(z).start()
-        pl.when(z == 0)(down_up)
+        pl.when(jnp.logical_or(z == 0, z == steps - 2))(down_up)
 
     total = 2 * rows
     lane = lax.broadcasted_iota(jnp.int32, (total, wide), 1)
@@ -176,6 +176,12 @@
             over(0, s - 2)
             next_above(0)
 
+        @pl.when(jnp.logical_and(d == 2, z == steps - 1))
+        def _():
+            for c in (1, 2):
+                await_chunk(c, s - 2)
+                over(c, s - 2)
+
         kv_forward(j).wait_recv()
 
         @pl.when(has_up)
@@ -185,7 +191,8 @@
             @pl.when(j == 0)
             def _():
                 onward(0, s - 2, above)
-                pl.when(z == 1)(down_up)
+                if steps != 3:
+                    pl.when(z == 1)(down_up)
 
         @pl.when(d == 1)
         def _():
@@ -237,7 +244,7 @@
         @pl.when(z - d >= 0)
         def _():
             arrive(0, s - 2 * d, above, has_up)
-            pl.when(jnp.logical_and(d == z, has_up))(down_up)
+            pl.when(jnp.logical_and(d == z, z < steps - 2))(down_up)
 
     @pl.when(z == 0)
     def _():
@@ -305,7 +312,7 @@
             arrive(1, 2 * i + y, above, has_up)
             arrive(2, 2 * i + y, above, has_up)
 
-    down_below(z - 1)
+    pl.when(jnp.logical_or(z < steps - 1, z < 2))(lambda: down_below(z - 1))
     pair_depth = 2 * up_ref.shape[0]
     hsum[...] = jnp.zeros_like(hsum)
 

time: 139 us -> 136 us (0.978)
  Pallas kernels: 136 us -> 132 us
    pallas_call x1, Pallas kernels: 136 us -> 132 us  [per_device(): pl.pallas_call(functools.partial(layer_kernel, n, tp), out_shape=jax.Shap...]
where the time goes in v5:
time: 136 us; the launch traced here: 134 us
  Pallas kernels  132 us (97%)
  local copies, waits for them, and re-layouts  1.88 us (1%)
    pallas_call x1, Pallas kernels, per_device(): pl.pallas_call(functools.partial(layer_kernel, n, tp), out_shape=jax.Shap...  132 us

profile of v5, /device:TPU:25, one launch (start us, length us, event | category | flops | bytes accessed | tf_op | source)
XLA Modules:
  0.0 134.2 jit_solution(9213179019359941029)
XLA Ops:
  0.0 132.3 %shard_map.100 = bf16[128,2048]{1,0:T(8,128)(2,1)} custom-call(f32[2]{0:T(128)} %lam_ref.1, bf16[512,256]{1,0:T(8,128)(2,1)} %q_ref.1, bf16[512,256]{1,0:T(8,128)(2,1)} %k_ref.1, bf16[512,256]{1,0:T(8,128)(2,1)} %v_ref.1, f32[1,128]{1,0:T(1,128)} %bitcast.3, bf16[256,1024]{1,0:T(8,128)(2,1)} %up_ref.1, bf16[1024,256]{1,0:T(8,128)(2,1)} %dn_ref.1, ...), custom_call_target="tpu_custom_call" | custom-call | tf_op jit(solution)/shard_map/pallas_call | solution.py:417
  132.3 1.9 %copy.12 = bf16[128,2048]{1,0:T(8,128)(2,1)} copy(bf16[128,2048]{1,0:T(8,128)(2,1)} %shard_map.100) | data formatting | bytes 1048576
